TPU v7x, 32 devices: a whole 2x2x4 slice. The times are simulated.
32 devices in a mesh: grp: 2 (over y), dp: 2 (over x), kv: 4 (over z), tp: 2 (over core).
Axes of the slice: x: 2, y: 2, z: 4, core: 2. Of those that a mesh axis runs over, the one named last changes fastest.
Arguments:
- inputs: bfloat16 [32, 4096], P(('grp', 'dp'), 'kv'), parts along dimension 0, may hold values from -6 to 6
- gain_in: float32 [4096], P('kv'), may hold values from 0.1 to 1.9
- w_gate: bfloat16 [4096, 2048], P('kv', 'tp'), may hold values from -0.09375 to 0.09375
- w_input: bfloat16 [4096, 2048], P('kv', 'tp'), may hold values from -0.09375 to 0.09375
- w_bproj: bfloat16 [4096, 1024], P('kv', 'tp'), may hold values from -0.09375 to 0.09375
- w_cproj: bfloat16 [4096, 1024], P('kv', 'tp'), may hold values from -0.09375 to 0.09375
- w_step: bfloat16 [4096, 32], P('kv', 'tp'), may hold values from -0.09375 to 0.09375
- conv_input: float32 [4, 2048], P(None, 'tp'), may hold values from -3 to 3
- conv_bproj: float32 [4, 1024], P(None, 'tp'), may hold values from -3 to 3
- conv_cproj: float32 [4, 1024], P(None, 'tp'), may hold values from -3 to 3
- tail_input: bfloat16 [32, 3, 2048], P(('grp', 'dp', 'kv'), None, 'tp'), parts along dimension 0, may hold values from -6 to 6
- tail_bproj: bfloat16 [32, 3, 1024], P(('grp', 'dp', 'kv'), None, 'tp'), parts along dimension 0, may hold values from -6 to 6
- tail_cproj: bfloat16 [32, 3, 1024], P(('grp', 'dp', 'kv'), None, 'tp'), parts along dimension 0, may hold values from -6 to 6
- step_bias: float32 [32], P('tp'), may hold values from -3 to 0
- decay_log: float32 [32], P('tp'), may hold values from -2 to 2
- block_input: bfloat16 [32, 128, 2048], P(('grp', 'dp', 'kv'), None, 'tp'), parts along dimension 0, may hold values from -6 to 6
- block_bproj: bfloat16 [32, 128, 1024], P(('grp', 'dp', 'kv'), None, 'tp'), parts along dimension 0, may hold values from -0.59765625 to 0.59765625
- block_step: float32 [32, 128, 32], P(('grp', 'dp', 'kv'), None, 'tp'), parts along dimension 0, may hold values from 0.005 to 0.2
- lengths: int32 [32], P(('grp', 'dp', 'kv')), parts along dimension 0, may hold values from 1 to 127, 512 in all
- state: float32 [32, 32, 64, 128], P(('grp', 'dp', 'kv'), 'tp'), parts along dimension 0, may hold values from -0.6 to 0.6
- gain_mix: float32 [2048], P('tp'), may hold values from 0.1 to 1.9
- w_out: bfloat16 [2048, 4096], P('tp', 'kv'), may hold values from -0.125 to 0.125
- gain_mlp: float32 [4096], P(('kv', 'tp')), may hold values from 0.1 to 1.9
- w_up: bfloat16 [4096, 16384], P(('kv', 'tp'), 'dp'), may hold values from -0.09375 to 0.09375
- w_down: bfloat16 [16384, 4096], P('dp', ('kv', 'tp')), may hold values from -0.046875 to 0.046875
Outputs:
- layer_out: bfloat16 [32, 4096], P(('grp', 'dp'), ('kv', 'tp')), parts along dimension 0
There are 2 independent parts, one for each index of `grp`. A program takes and returns all parts, laid end to end along the dimension named above; an argument that names none is the same for every part. Nothing has to cross between parts.
Inputs may be any that keep to these rules, and one draw needn't show every extreme that they name: `lengths`: the number of live positions before the new token in each sequence's current block; the largest equals 127 in every draw.
All inputs are finite; a program needn't handle non-finite values.
Results may differ from a plain program's by a relative error of at most 0.012.
Values may be sent and summed in bfloat16 or wider, within the bound.
A program may use at most 64 MiB of HBM per device.

v0:
```python
import jax
import jax.numpy as jnp
from jax import lax
from jax.sharding import PartitionSpec as P

D = 4096
HEAD_DIM = 64
D_STATE = 128
TAPS = 4
SSM_WIDTH = 2048
EPS = 1e-06


def convolve(history, weights, newest):
    summed = weights[TAPS - 1] * newest
    for offset in range(TAPS - 1):
        summed = summed + weights[offset] * history[:, offset].astype(jnp.float32)
    return jax.nn.silu(summed)


def per_device(
    inputs,
    gain_in,
    w_gate,
    w_input,
    w_bproj,
    w_cproj,
    w_step,
    conv_input,
    conv_bproj,
    conv_cproj,
    tail_input,
    tail_bproj,
    tail_cproj,
    step_bias,
    decay_log,
    block_input,
    block_bproj,
    block_step,
    lengths,
    state,
    gain_mix,
    w_out,
    gain_mlp,
    w_up,
    w_down,
):
    stream = inputs.astype(jnp.float32)
    squares = jnp.sum(stream * stream, axis=1)
    scaled = (stream * gain_in).astype(jnp.bfloat16)
    matrices = (w_gate, w_input, w_bproj, w_cproj, w_step)
    pieces = [jnp.dot(scaled, weight, preferred_element_type=jnp.float32) for weight in matrices]
    projected, totals = (
        lax.psum_scatter(jnp.concatenate(pieces, axis=1), "kv", scatter_dimension=0, tiled=True),
        lax.psum_scatter(squares, "kv", scatter_dimension=0, tiled=True),
    )
    inverse = lax.rsqrt(totals / D + EPS)[:, None]
    bounds = [0]
    for weight in matrices:
        bounds.append(bounds[-1] + weight.shape[1])
    gate_pre, value_pre, b_pre, c_pre, step_pre = [
        projected[:, bounds[member] : bounds[member + 1]] * inverse for member in range(5)
    ]
    seq_count = lengths.shape[0]
    head_count = step_bias.shape[0]
    group_count = w_bproj.shape[1] // D_STATE
    block_len = block_step.shape[1]
    per_group = head_count // group_count
    current = convolve(tail_input, conv_input, value_pre)
    b_now = convolve(tail_bproj, conv_bproj, b_pre)
    c_now = convolve(tail_cproj, conv_cproj, c_pre)
    step_size = jax.nn.softplus(step_pre + step_bias)
    decay_rate = -jnp.exp(decay_log)
    positions = lax.broadcasted_iota(jnp.int32, (1, block_len), 1)
    live_rows = (positions < lengths[:, None]).astype(jnp.float32)
    masked = block_step * live_rows[:, :, None]
    later_steps = jnp.sum(masked, axis=1, keepdims=True) - jnp.cumsum(masked, axis=1)
    decays = jnp.exp(decay_rate * (step_size[:, None, :] + later_steps)) * live_rows[:, :, None]
    c_query = c_now.astype(jnp.bfloat16).reshape(seq_count, group_count, D_STATE)
    keys = block_bproj.reshape(seq_count, block_len, group_count, D_STATE)
    scores = jnp.einsum("bsgn,bgn->bsg", keys, c_query, preferred_element_type=jnp.float32)
    scores = jnp.repeat(scores, per_group, axis=2)
    weights = (decays * scores * block_step).astype(jnp.bfloat16)
    values = block_input.reshape(seq_count, block_len, head_count, HEAD_DIM)
    inner_sum = jnp.einsum("bsh,bshp->bhp", weights, values, preferred_element_type=jnp.float32)
    c_full = c_now.reshape(seq_count, group_count, D_STATE)
    b_full = b_now.reshape(seq_count, group_count, D_STATE)
    own_score = jnp.repeat(jnp.sum(c_full * b_full, axis=2), per_group, axis=1)
    own_term = (step_size * own_score)[:, :, None] * current.reshape(
        seq_count, head_count, HEAD_DIM
    )
    carried = jnp.exp(decay_rate * (step_size + jnp.sum(masked, axis=1)))
    c_heads = jnp.repeat(c_full, per_group, axis=1)
    readout = jnp.einsum("bhpn,bhn->bhp", state, c_heads, precision=lax.Precision.HIGHEST)
    mixed = (inner_sum + own_term + carried[:, :, None] * readout).reshape(
        seq_count, -1
    ) * jax.nn.silu(gate_pre)
    local_sq = jnp.sum(mixed * mixed, axis=1)
    total_sq = lax.psum(local_sq, "tp")
    normed = (mixed * lax.rsqrt(total_sq / SSM_WIDTH + EPS)[:, None] * gain_mix).astype(
        jnp.bfloat16
    )
    products = jnp.dot(
        lax.all_gather(normed, "kv", axis=0, tiled=True), w_out, preferred_element_type=jnp.float32
    )
    mixed_in = lax.psum_scatter(products, "tp", scatter_dimension=1, tiled=True)
    column_count = mixed_in.shape[1]
    residual = lax.dynamic_slice_in_dim(
        stream, lax.axis_index("tp") * column_count, column_count, 1
    )
    hidden = (residual + mixed_in).astype(jnp.bfloat16)
    lifted = (hidden.astype(jnp.float32) * gain_mlp).astype(jnp.bfloat16)
    all_lifted, all_hidden = (
        lax.all_gather(lifted, "dp", axis=0, tiled=True),
        lax.all_gather(hidden, "dp", axis=0, tiled=True),
    )
    whole_rows = all_hidden.astype(jnp.float32)
    row_sq = jnp.sum(whole_rows * whole_rows, axis=1)
    partial_value = jnp.dot(all_lifted, w_up, preferred_element_type=jnp.float32)
    sq_sum = lax.psum(row_sq, ("kv", "tp"))
    shares = lax.psum_scatter(partial_value, ("kv", "tp"), scatter_dimension=1, tiled=True)
    unit_share = jnp.square(jax.nn.relu(shares * lax.rsqrt(sq_sum / D + EPS)[:, None])).astype(
        jnp.bfloat16
    )
    hidden_units = lax.all_gather(unit_share, ("kv", "tp"), axis=1, tiled=True)
    lowered = lax.psum_scatter(
        jnp.dot(hidden_units, w_down, preferred_element_type=jnp.float32),
        "dp",
        scatter_dimension=0,
        tiled=True,
    )
    return (hidden.astype(jnp.float32) + lowered).astype(jnp.bfloat16)


def solution(mesh):
    return jax.shard_map(
        per_device,
        mesh=mesh,
        in_specs=(
            P(("grp", "dp"), "kv"),
            P("kv"),
            P("kv", "tp"),
            P("kv", "tp"),
            P("kv", "tp"),
            P("kv", "tp"),
            P("kv", "tp"),
            P(None, "tp"),
            P(None, "tp"),
            P(None, "tp"),
            P(("grp", "dp", "kv"), None, "tp"),
            P(("grp", "dp", "kv"), None, "tp"),
            P(("grp", "dp", "kv"), None, "tp"),
            P("tp"),
            P("tp"),
            P(("grp", "dp", "kv"), None, "tp"),
            P(("grp", "dp", "kv"), None, "tp"),
            P(("grp", "dp", "kv"), None, "tp"),
            P(("grp", "dp", "kv")),
            P(("grp", "dp", "kv"), "tp", None, None),
            P("tp"),
            P("tp", "kv"),
            P(("kv", "tp")),
            P(("kv", "tp"), "dp"),
            P("dp", ("kv", "tp")),
        ),
        out_specs=P(("grp", "dp"), ("kv", "tp")),
        check_vma=False,
    )
```

profile of v0, /device:TPU:0, one launch (start us, length us, event | category | flops | bytes accessed | tf_op | source)
XLA Modules:
  0.0 172.6 jit_solution(11683976073686166705)
XLA Ops:
  6.5 1.6 copy-done
  8.1 1.3 convolution_dynamic-update-slice_fusion.1
  10.4 0.7 copy-done.3
  11.4 0.6 copy-done.6
  12.3 14.1 %all-reduce.1 = f32[8]{0:T(128)} all-reduce(f32[8]{0:T(128)S(1)} %multiply_reduce_fusion.1), channel_id=3, replica_groups=mesh['grp'=2,'dp'=2,'kv'=4,'tp'=2] {'kv'}, use_global_device_ids=true, to_apply=%region_2.0.clone | all-reduce | flops 8 | bytes 64
  26.4 0.6 fusion.26
  27.6 1.1 copy.43
  28.7 0.8 copy.32
  29.5 1.3 compare_convert_fusion
  30.8 1.2 exponential_negate_fusion
  32.0 2.0 %copy.35 = bf16[2,128,1024]{1,2,0:T(8,128)(2,1)} copy(bf16[2,128,1024]{2,1,0:T(8,128)(2,1)} %param.40) | data formatting | bytes 1048576 | tf_op args[15]
  34.0 1.5 fusion.24
  35.5 1.3 dynamic-slice
  37.4 1.9 %fusion.22 = (f32[2,16]{1,0:T(2,128)}, f32[2,128,16]{2,1,0:T(8,128)}) fusion(f32[2,128,16]{2,1,0:T(8,128)S(1)} %copy.32, f32[2,128]{1,0:T(2,128)} %compare_convert_fusion), kind=kLoop, calls=%fused_computation.64 | loop fusion | flops 8160 | bytes 33920 | tf_op jit(solution)/shard_map/reduce_sum | solution.py:77
  39.3 1.7 reduce_window_sum.11
  41.0 1.3 fusion.19
  42.3 7.1 %all-reduce.4.cloned.1.call-done = f32[8,3088]{1,0:T(8,128)} async-done(((f32[8,3088]{1,0:T(8,128)}), f32[8,3088]{1,0:T(8,128)}) %all-reduce.4.cloned.1.call-update) | async-done | bytes 98832
  49.4 1.5 fusion.23
  50.9 1.3 reshape.87
  52.2 1.3 reshape.88
  53.5 0.8 multiply_reduce_fusion.3
  54.2 0.7 broadcast_in_dim.7
  54.9 1.3 reshape.89
  56.2 1.3 reshape.111
  57.5 0.9 fusion.27
  58.5 0.8 fusion.21
  59.3 0.7 multiply_exponential_fusion
  59.9 1.0 fusion
  61.1 0.9 divide_multiply_fusion.1
  62.1 1.4 fusion.28
  63.5 0.7 broadcast_in_dim.8
  64.2 1.7 %fusion.29 = f32[2,16,1,64]{3,2,1,0:T(1,128)S(1)} fusion(f32[2,16,128,1]{2,3,1,0:T(1,128)S(1)} %bitcast.82, f32[2,16,64,128]{3,2,1,0:T(8,128)S(1)} %copy-done.4), kind=kOutput, calls=%fused_computation.71 | convolution fusion | flops 3145728 | bytes 1073152 | tf_op jit(solution)/shard_map/bhpn,bhn->bhp/dot_general | solution.py:94
  66.1 1.0 multiply_reduce_fusion.2
  67.1 2.5 %psum.14 = f32[2]{0:T(128)S(1)} all-reduce(f32[2]{0:T(128)S(1)} %get-tuple-element.7), channel_id=1, replica_groups=mesh['grp'=2,'dp'=2,'kv'=4,'tp'=2] {'tp'}, use_global_device_ids=true, to_apply=%region_7.8 | all-reduce | flops 2 | bytes 16 | tf_op jit(solution)/shard_map/psum | solution.py:99
  69.6 13.2 %all-gather = bf16[4,2,1024]{2,1,0:T(2,128)(2,1)S(1)} all-gather(bf16[1,2,1024]{2,1,0:T(2,128)(2,1)S(1)} %fusion.16), channel_id=1, replica_groups=mesh['grp'=2,'dp'=2,'kv'=4,'tp'=2] {'kv'}, dimensions={0}, use_global_device_ids=true | all-gather | bytes 20480 | tf_op jit(solution)/shard_map/all_gather | solution.py:104
  82.8 2.6 %fusion.30 = f32[8,1024]{1,0:T(8,128)} fusion(bf16[8,1024]{1,0:T(8,128)(2,1)S(1)} %reshape.103, bf16[1024,1024]{1,0:T(8,128)(2,1)} %param.46), kind=kOutput, calls=%fused_computation.72 | convolution fusion | flops 16777216 | bytes 2146304 | tf_op jit(solution)/shard_map/dot_general | solution.py:103
  85.5 7.6 %reduce-scatter.4.cloned.1.call-done = f32[8,512]{1,0:T(8,128)} async-done(((f32[8,1024]{1,0:T(8,128)}), f32[8,512]{1,0:T(8,128)}) %reduce-scatter.4.cloned.1.call-update) | async-done | bytes 16400 | tf_op jit(solution)/shard_map/reduce_scatter | solution.py:106
  93.1 0.7 fusion.1
  93.9 4.3 %all_gather.13 = bf16[16,512]{1,0:T(8,128)(2,1)S(1)} all-gather(bf16[8,512]{1,0:T(8,128)(2,1)S(1)} %get-tuple-element.5), channel_id=1, replica_groups=mesh['grp'=2,'dp'=2,'kv'=4,'tp'=2] {'dp'}, dimensions={0}, use_global_device_ids=true | all-gather | bytes 24576 | tf_op jit(solution)/shard_map/all_gather | solution.py:114
  98.2 5.4 %fusion.31 = f32[16,8192]{1,0:T(8,128)} fusion(bf16[16,512]{1,0:T(8,128)(2,1)S(1)} %all_gather.13, bf16[512,8192]{1,0:T(8,128)(2,1)} %param.48), kind=kOutput, calls=%fused_computation.73 | convolution fusion | flops 134217728 | bytes 8929280 | tf_op jit(solution)/shard_map/dot_general | solution.py:119
  103.7 4.4 %all_gather.14 = bf16[16,512]{1,0:T(8,128)(2,1)S(1)} all-gather(bf16[8,512]{1,0:T(8,128)(2,1)S(1)} %get-tuple-element.6), channel_id=1, replica_groups=mesh['grp'=2,'dp'=2,'kv'=4,'tp'=2] {'dp'}, dimensions={0}, use_global_device_ids=true | all-gather | bytes 24576 | tf_op jit(solution)/shard_map/all_gather | solution.py:115
  108.1 14.8 %psum.15 = f32[16]{0:T(128)S(1)} all-reduce(f32[16]{0:T(128)S(1)} %multiply_reduce_fusion), channel_id=1, replica_groups=mesh['grp'=2,'dp'=2,'kv'=4,'tp'=2] {'kv','tp'}, use_global_device_ids=true, to_apply=%region_11.12 | all-reduce | flops 16 | bytes 128 | tf_op jit(solution)/shard_map/psum | solution.py:120
  123.0 13.2 %reduce-scatter.6.cloned.1.call-done = f32[16,1024]{1,0:T(8,128)} async-done(((f32[16,8192]{1,0:T(8,128)}), f32[16,1024]{1,0:T(8,128)}) %reduce-scatter.6.cloned.1.call-update) | async-done | bytes 65552 | tf_op jit(solution)/shard_map/reduce_scatter | solution.py:121
  136.2 0.9 multiply_convert_fusion.1
  137.1 14.2 %all_gather.15 = bf16[16,8192]{1,0:T(8,128)(2,1)S(1)} all-gather(bf16[16,1024]{1,0:T(8,128)(2,1)S(1)} %multiply_convert_fusion.1), channel_id=1, replica_groups=mesh['grp'=2,'dp'=2,'kv'=4,'tp'=2] {'kv','tp'}, dimensions={1}, use_global_device_ids=true | all-gather | bytes 294912 | tf_op jit(solution)/shard_map/all_gather | solution.py:125
  151.3 5.2 %fusion.32 = f32[16,512]{1,0:T(8,128)} fusion(bf16[16,8192]{1,0:T(8,128)(2,1)S(1)} %all_gather.15, bf16[8192,512]{1,0:T(8,128)(2,1)} %param.49), kind=kOutput, calls=%fused_computation.74 | convolution fusion | flops 134217728 | bytes 8683520 | tf_op jit(solution)/shard_map/dot_general | solution.py:127
  156.5 8.3 %reduce-scatter.8.cloned.1.call-done = f32[8,512]{1,0:T(8,128)} async-done(((f32[16,512]{1,0:T(8,128)}), f32[8,512]{1,0:T(8,128)}) %reduce-scatter.8.cloned.1.call-update) | async-done | bytes 16400 | tf_op jit(solution)/shard_map/reduce_scatter | solution.py:126
  164.8 1.3 fusion.2
  (51 shorter events, 3.0 us)
Async XLA Ops:
  6.5 1.6 copy-start
  6.5 2.9 %copy-start.5 = (bf16[8,1024]{1,0:T(8,128)(2,1)S(1)}, bf16[8,1024]{1,0:T(8,128)(2,1)}, u32[]{:S(2)}) copy-start(bf16[8,1024]{1,0:T(8,128)(2,1)} %param.25) | copy-start | bytes 49156
  6.5 2.9 %copy-start.7 = (f32[1024]{0:T(1024)S(1)}, f32[1024]{0:T(1024)}, u32[]{:S(2)}) copy-start(f32[1024]{0:T(1024)} %param.26) | copy-start | bytes 12292
  6.5 42.8 %all-reduce.4.cloned.1.call-start = ((), (), s32[]{:S(2)}) async-start(), calls=%async_computation.6 | async-start | bytes 204800
  8.1 1.6 copy-start.1
  8.1 2.0 %copy-start.2 = (bf16[1024,512]{1,0:T(8,128)(2,1)S(1)}, bf16[1024,512]{1,0:T(8,128)(2,1)}, u32[]{:S(2)}) copy-start(bf16[1024,512]{1,0:T(8,128)(2,1)} %param.29) | copy-start | bytes 3145732
  9.8 1.3 copy-start.3
  9.8 1.5 copy-start.8
  9.8 16.6 %copy-start.10 = (f32[4,512]{1,0:T(4,128)S(1)}, f32[4,512]{1,0:T(4,128)}, u32[]{:S(2)}) copy-start(f32[4,512]{1,0:T(4,128)} %param.34) | copy-start | bytes 24580
  9.8 17.3 %copy-start.11 = (f32[4,512]{1,0:T(4,128)S(1)}, f32[4,512]{1,0:T(4,128)}, u32[]{:S(2)}) copy-start(f32[4,512]{1,0:T(4,128)} %param.33) | copy-start | bytes 24580
  11.4 0.6 copy-start.6
  12.1 52.1 %copy-start.4 = (f32[2,16,64,128]{3,2,1,0:T(8,128)S(1)}, f32[2,16,64,128]{3,2,1,0:T(8,128)}, u32[]{:S(2)}) copy-start(f32[2,16,64,128]{3,2,1,0:T(8,128)} %param.44) | copy-start | bytes 3145732
  12.1 81.0 %reduce-scatter.4.cloned.1.call-start = ((), (), s32[]{:S(2)}) async-start(), calls=%async_computation.3 | async-start | bytes 49152 | tf_op jit(solution)/shard_map/reduce_scatter | solution.py:106
  58.3 7.7 %copy-start.9 = (f32[2]{0:T(128)S(1)}, f32[2]{0:T(128)}, u32[]{:S(2)}) copy-start(f32[2]{0:T(128)} %fusion.19) | copy-start | bytes 28
  58.3 11.2 %copy-start.12 = (f32[1024]{0:T(1024)S(1)}, f32[1024]{0:T(1024)}, u32[]{:S(2)}) copy-start(f32[1024]{0:T(1024)} %param.45) | copy-start | bytes 12292
  61.1 32.1 %copy-start.13 = (f32[512]{0:T(512)S(1)}, f32[512]{0:T(512)}, u32[]{:S(2)}) copy-start(f32[512]{0:T(512)} %param.47) | copy-start | bytes 6148
  85.5 50.8 %reduce-scatter.6.cloned.1.call-start = ((), (), s32[]{:S(2)}) async-start(), calls=%async_computation.4 | async-start | bytes 589824 | tf_op jit(solution)/shard_map/reduce_scatter | solution.py:121
  103.6 61.2 %reduce-scatter.8.cloned.1.call-start = ((), (), s32[]{:S(2)}) async-start(), calls=%async_computation.5 | async-start | bytes 49152 | tf_op jit(solution)/shard_map/reduce_scatter | solution.py:126
Sparse Core Ops, SparseCore 0:
  12.2 37.1 all-reduce.3
  85.6 7.5 reduce-scatter.3
  103.7 32.4 reduce-scatter.5
  156.6 8.0 reduce-scatter.7
where the time goes:
time: 174 us; the launch traced here: 173 us
  blocking collectives  67.6 us (39%)
  waiting for transfers between devices  36.2 us (21%)
  matrix products  19.4 us (11%)
  local copies, waits for them, and re-layouts  18.1 us (10%)
  other arithmetic  17.4 us (10%)
  between operations  13.9 us (8%)
    psum x1, blocking collectives, per_device(): sq_sum = lax.psum(row_sq, ('kv', 'tp'))  14.8 us
    all_gather x1, blocking collectives, per_device(): hidden_units = lax.all_gather(unit_share, ('kv', 'tp'), axis=1, tiled=True)  14.2 us
    unnamed x1, blocking collectives  14.1 us
    all_gather x1, blocking collectives, per_device(): lax.all_gather(normed, 'kv', axis=0, tiled=True)  13.2 us
    reduce_scatter x1, waiting for transfers between devices, per_device(): lax.psum_scatter(partial_value, ('kv', 'tp'), scatter_dimension=1, tiled=...  13.2 us
    reduce_scatter x1, waiting for transfers between devices, per_device(): lax.psum_scatter(jnp.dot(hidden_units, w_down, preferred_element_type=jnp...  8.27 us
    reduce_scatter x1, waiting for transfers between devices, per_device(): mixed_in = lax.psum_scatter(products, 'tp', scatter_dimension=1, tiled=True)  7.61 us
    unnamed x32, local copies, waits for them, and re-layouts  7.41 us
  transfers between devices with their start and end apart: 4, of which 4 were waited for; matrix products, arithmetic and copies ran while one was open for 9% of the time, Pallas kernels for 0%

commit v1 on v0

--- a/solution.py
+++ b/solution.py
@@ -122,7 +122,8 @@
     unit_share = jnp.square(jax.nn.relu(shares * lax.rsqrt(sq_sum / D + EPS)[:, None])).astype(
         jnp.bfloat16
     )
-    hidden_units = lax.all_gather(unit_share, ("kv", "tp"), axis=1, tiled=True)
+    shards = lax.all_gather(unit_share, ("kv", "tp"))
+    hidden_units = jnp.concatenate(shards, axis=1)
     lowered = lax.psum_scatter(
         jnp.dot(hidden_units, w_down, preferred_element_type=jnp.float32),
         "dp",

time: 174 us -> 174 us (level)
    unnamed x32 -> x33, local copies, waits for them, and re-layouts: 7.41 us -> 7.43 us
where the time goes in v1:
time: 174 us; the launch traced here: 173 us
  blocking collectives  67.6 us (39%)
  waiting for transfers between devices  36.2 us (21%)
  matrix products  19.4 us (11%)
  local copies, waits for them, and re-layouts  18.1 us (10%)
  other arithmetic  17.4 us (10%)
  between operations  13.9 us (8%)
    psum x1, blocking collectives, per_device(): sq_sum = lax.psum(row_sq, ('kv', 'tp'))  14.8 us
    all_gather x1, blocking collectives, per_device(): shards = lax.all_gather(unit_share, ('kv', 'tp'))  14.2 us
    unnamed x1, blocking collectives  14.1 us
    all_gather x1, blocking collectives, per_device(): lax.all_gather(normed, 'kv', axis=0, tiled=True)  13.2 us
    reduce_scatter x1, waiting for transfers between devices, per_device(): lax.psum_scatter(partial_value, ('kv', 'tp'), scatter_dimension=1, tiled=...  13.2 us
    reduce_scatter x1, waiting for transfers between devices, per_device(): lax.psum_scatter(jnp.dot(hidden_units, w_down, preferred_element_type=jnp...  8.27 us
    reduce_scatter x1, waiting for transfers between devices, per_device(): mixed_in = lax.psum_scatter(products, 'tp', scatter_dimension=1, tiled=True)  7.61 us
    unnamed x33, local copies, waits for them, and re-layouts  7.43 us
  transfers between devices with their start and end apart: 4, of which 4 were waited for; matrix products, arithmetic and copies ran while one was open for 9% of the time, Pallas kernels for 0%

profile of v1, /device:TPU:0, one launch (start us, length us, event | category | flops | bytes accessed | tf_op | source)
XLA Modules:
  0.0 172.7 jit_solution(7608849386855593714)
XLA Ops:
  6.5 1.6 copy-done
  8.1 1.3 convolution_dynamic-update-slice_fusion.1
  10.4 0.7 copy-done.3
  11.4 0.6 copy-done.6
  12.3 14.1 %all-reduce.1 = f32[8]{0:T(128)} all-reduce(f32[8]{0:T(128)S(1)} %multiply_reduce_fusion.1), channel_id=4, replica_groups=mesh['grp'=2,'dp'=2,'kv'=4,'tp'=2] {'kv'}, use_global_device_ids=true, to_apply=%region_2.0.clone | all-reduce | flops 8 | bytes 64
  26.4 0.6 fusion.26
  27.6 1.1 copy.45
  28.7 0.8 copy.33
  29.5 1.3 compare_convert_fusion
  30.8 1.2 exponential_negate_fusion
  32.0 2.0 %copy.36 = bf16[2,128,1024]{1,2,0:T(8,128)(2,1)} copy(bf16[2,128,1024]{2,1,0:T(8,128)(2,1)} %param.40) | data formatting | bytes 1048576 | tf_op args[15]
  34.0 1.5 fusion.24
  35.5 1.3 dynamic-slice
  37.4 1.9 %fusion.22 = (f32[2,16]{1,0:T(2,128)}, f32[2,128,16]{2,1,0:T(8,128)}) fusion(f32[2,128,16]{2,1,0:T(8,128)S(1)} %copy.33, f32[2,128]{1,0:T(2,128)} %compare_convert_fusion), kind=kLoop, calls=%fused_computation.64 | loop fusion | flops 8160 | bytes 33920 | tf_op jit(solution)/shard_map/reduce_sum | solution.py:77
  39.3 1.7 reduce_window_sum.11
  41.0 1.3 fusion.19
  42.3 7.1 %all-reduce.4.cloned.1.call-done = f32[8,3088]{1,0:T(8,128)} async-done(((f32[8,3088]{1,0:T(8,128)}), f32[8,3088]{1,0:T(8,128)}) %all-reduce.4.cloned.1.call-update) | async-done | bytes 98832
  49.4 1.5 fusion.23
  50.9 1.3 reshape.93
  52.2 1.3 reshape.94
  53.5 0.8 multiply_reduce_fusion.3
  54.2 0.7 broadcast_in_dim.7
  54.9 1.3 reshape.95
  56.2 1.3 reshape.120
  57.5 0.9 fusion.27
  58.5 0.8 fusion.21
  59.3 0.7 multiply_exponential_fusion
  59.9 1.0 fusion
  61.1 0.9 divide_multiply_fusion.1
  62.1 1.4 fusion.28
  63.5 0.7 broadcast_in_dim.8
  64.2 1.7 %fusion.29 = f32[2,16,1,64]{3,2,1,0:T(1,128)S(1)} fusion(f32[2,16,128,1]{2,3,1,0:T(1,128)S(1)} %bitcast.90, f32[2,16,64,128]{3,2,1,0:T(8,128)S(1)} %copy-done.4), kind=kOutput, calls=%fused_computation.71 | convolution fusion | flops 3145728 | bytes 1073152 | tf_op jit(solution)/shard_map/bhpn,bhn->bhp/dot_general | solution.py:94
  66.1 1.0 multiply_reduce_fusion.2
  67.1 2.5 %psum.14 = f32[2]{0:T(128)S(1)} all-reduce(f32[2]{0:T(128)S(1)} %get-tuple-element.7), channel_id=1, replica_groups=mesh['grp'=2,'dp'=2,'kv'=4,'tp'=2] {'tp'}, use_global_device_ids=true, to_apply=%region_7.8 | all-reduce | flops 2 | bytes 16 | tf_op jit(solution)/shard_map/psum | solution.py:99
  69.6 13.2 %all-gather.1 = bf16[4,2,1024]{2,1,0:T(2,128)(2,1)S(1)} all-gather(bf16[1,2,1024]{2,1,0:T(2,128)(2,1)S(1)} %fusion.16), channel_id=1, replica_groups=mesh['grp'=2,'dp'=2,'kv'=4,'tp'=2] {'kv'}, dimensions={0}, use_global_device_ids=true | all-gather | bytes 20480 | tf_op jit(solution)/shard_map/all_gather | solution.py:104
  82.8 2.6 %fusion.30 = f32[8,1024]{1,0:T(8,128)} fusion(bf16[8,1024]{1,0:T(8,128)(2,1)S(1)} %reshape.112, bf16[1024,1024]{1,0:T(8,128)(2,1)} %param.46), kind=kOutput, calls=%fused_computation.72 | convolution fusion | flops 16777216 | bytes 2146304 | tf_op jit(solution)/shard_map/dot_general | solution.py:103
  85.5 7.6 %reduce-scatter.4.cloned.1.call-done = f32[8,512]{1,0:T(8,128)} async-done(((f32[8,1024]{1,0:T(8,128)}), f32[8,512]{1,0:T(8,128)}) %reduce-scatter.4.cloned.1.call-update) | async-done | bytes 16400 | tf_op jit(solution)/shard_map/reduce_scatter | solution.py:106
  93.1 0.7 fusion.1
  93.9 4.3 %all_gather.16 = bf16[16,512]{1,0:T(8,128)(2,1)S(1)} all-gather(bf16[8,512]{1,0:T(8,128)(2,1)S(1)} %get-tuple-element.5), channel_id=1, replica_groups=mesh['grp'=2,'dp'=2,'kv'=4,'tp'=2] {'dp'}, dimensions={0}, use_global_device_ids=true | all-gather | bytes 24576 | tf_op jit(solution)/shard_map/all_gather | solution.py:114
  98.2 5.4 %fusion.31 = f32[16,8192]{1,0:T(8,128)} fusion(bf16[16,512]{1,0:T(8,128)(2,1)S(1)} %all_gather.16, bf16[512,8192]{1,0:T(8,128)(2,1)} %param.48), kind=kOutput, calls=%fused_computation.73 | convolution fusion | flops 134217728 | bytes 8929280 | tf_op jit(solution)/shard_map/dot_general | solution.py:119
  103.7 4.4 %all_gather.17 = bf16[16,512]{1,0:T(8,128)(2,1)S(1)} all-gather(bf16[8,512]{1,0:T(8,128)(2,1)S(1)} %get-tuple-element.6), channel_id=1, replica_groups=mesh['grp'=2,'dp'=2,'kv'=4,'tp'=2] {'dp'}, dimensions={0}, use_global_device_ids=true | all-gather | bytes 24576 | tf_op jit(solution)/shard_map/all_gather | solution.py:115
  108.1 14.8 %psum.15 = f32[16]{0:T(128)S(1)} all-reduce(f32[16]{0:T(128)S(1)} %multiply_reduce_fusion), channel_id=1, replica_groups=mesh['grp'=2,'dp'=2,'kv'=4,'tp'=2] {'kv','tp'}, use_global_device_ids=true, to_apply=%region_11.12 | all-reduce | flops 16 | bytes 128 | tf_op jit(solution)/shard_map/psum | solution.py:120
  123.0 13.2 %reduce-scatter.6.cloned.1.call-done = f32[16,1024]{1,0:T(8,128)} async-done(((f32[16,8192]{1,0:T(8,128)}), f32[16,1024]{1,0:T(8,128)}) %reduce-scatter.6.cloned.1.call-update) | async-done | bytes 65552 | tf_op jit(solution)/shard_map/reduce_scatter | solution.py:121
  136.2 0.9 multiply_convert_fusion.1
  137.1 14.2 %all-gather = bf16[128,1024]{1,0:T(8,128)(2,1)S(1)} all-gather(bf16[16,1024]{1,0:T(8,128)(2,1)S(1)} %multiply_convert_fusion.1), channel_id=2, replica_groups=mesh['grp'=2,'dp'=2,'kv'=4,'tp'=2] {'kv','tp'}, dimensions={0}, use_global_device_ids=true | all-gather | bytes 294912 | tf_op jit(solution)/shard_map/all_gather | solution.py:125
  151.3 5.2 %fusion.32 = f32[16,512]{1,0:T(8,128)} fusion(bf16[16,8192]{1,0:T(8,128)(2,1)S(1)} %bitcast.86, bf16[8192,512]{1,0:T(8,128)(2,1)} %param.49), kind=kOutput, calls=%fused_computation.74 | convolution fusion | flops 134217728 | bytes 8683520 | tf_op jit(solution)/shard_map/dot_general | solution.py:128
  156.5 8.3 %reduce-scatter.8.cloned.1.call-done = f32[8,512]{1,0:T(8,128)} async-done(((f32[16,512]{1,0:T(8,128)}), f32[8,512]{1,0:T(8,128)}) %reduce-scatter.8.cloned.1.call-update) | async-done | bytes 16400 | tf_op jit(solution)/shard_map/reduce_scatter | solution.py:127
  164.8 1.3 fusion.2
  (52 shorter events, 3.0 us)
Async XLA Ops:
  6.5 1.6 copy-start
  6.5 2.9 %copy-start.5 = (bf16[8,1024]{1,0:T(8,128)(2,1)S(1)}, bf16[8,1024]{1,0:T(8,128)(2,1)}, u32[]{:S(2)}) copy-start(bf16[8,1024]{1,0:T(8,128)(2,1)} %param.25) | copy-start | bytes 49156
  6.5 2.9 %copy-start.7 = (f32[1024]{0:T(1024)S(1)}, f32[1024]{0:T(1024)}, u32[]{:S(2)}) copy-start(f32[1024]{0:T(1024)} %param.26) | copy-start | bytes 12292
  6.5 42.8 %all-reduce.4.cloned.1.call-start = ((), (), s32[]{:S(2)}) async-start(), calls=%async_computation.6 | async-start | bytes 204800
  8.1 1.6 copy-start.1
  8.1 2.0 %copy-start.2 = (bf16[1024,512]{1,0:T(8,128)(2,1)S(1)}, bf16[1024,512]{1,0:T(8,128)(2,1)}, u32[]{:S(2)}) copy-start(bf16[1024,512]{1,0:T(8,128)(2,1)} %param.29) | copy-start | bytes 3145732
  9.8 1.3 copy-start.3
  9.8 1.5 copy-start.8
  9.8 16.6 %copy-start.10 = (f32[4,512]{1,0:T(4,128)S(1)}, f32[4,512]{1,0:T(4,128)}, u32[]{:S(2)}) copy-start(f32[4,512]{1,0:T(4,128)} %param.34) | copy-start | bytes 24580
  9.8 17.3 %copy-start.11 = (f32[4,512]{1,0:T(4,128)S(1)}, f32[4,512]{1,0:T(4,128)}, u32[]{:S(2)}) copy-start(f32[4,512]{1,0:T(4,128)} %param.33) | copy-start | bytes 24580
  11.4 0.6 copy-start.6
  12.1 52.1 %copy-start.4 = (f32[2,16,64,128]{3,2,1,0:T(8,128)S(1)}, f32[2,16,64,128]{3,2,1,0:T(8,128)}, u32[]{:S(2)}) copy-start(f32[2,16,64,128]{3,2,1,0:T(8,128)} %param.44) | copy-start | bytes 3145732
  12.1 81.0 %reduce-scatter.4.cloned.1.call-start = ((), (), s32[]{:S(2)}) async-start(), calls=%async_computation.3 | async-start | bytes 49152 | tf_op jit(solution)/shard_map/reduce_scatter | solution.py:106
  58.3 7.7 %copy-start.9 = (f32[2]{0:T(128)S(1)}, f32[2]{0:T(128)}, u32[]{:S(2)}) copy-start(f32[2]{0:T(128)} %fusion.19) | copy-start | bytes 28
  58.3 11.2 %copy-start.12 = (f32[1024]{0:T(1024)S(1)}, f32[1024]{0:T(1024)}, u32[]{:S(2)}) copy-start(f32[1024]{0:T(1024)} %param.45) | copy-start | bytes 12292
  61.1 32.1 %copy-start.13 = (f32[512]{0:T(512)S(1)}, f32[512]{0:T(512)}, u32[]{:S(2)}) copy-start(f32[512]{0:T(512)} %param.47) | copy-start | bytes 6148
  85.5 50.8 %reduce-scatter.6.cloned.1.call-start = ((), (), s32[]{:S(2)}) async-start(), calls=%async_computation.4 | async-start | bytes 589824 | tf_op jit(solution)/shard_map/reduce_scatter | solution.py:121
  103.6 61.2 %reduce-scatter.8.cloned.1.call-start = ((), (), s32[]{:S(2)}) async-start(), calls=%async_computation.5 | async-start | bytes 49152 | tf_op jit(solution)/shard_map/reduce_scatter | solution.py:127
Sparse Core Ops, SparseCore 0:
  12.2 37.1 all-reduce.3
  85.6 7.5 reduce-scatter.3
  103.7 32.4 reduce-scatter.5
  156.7 8.0 reduce-scatter.7
